TPU v7x, 32 devices: a whole 2x2x4 slice. The times are simulated.
32 devices in a mesh: sp: 8 (over z, x), tp: 4 (over y, core).
Axes of the slice: x: 2, y: 2, z: 4, core: 2. Of those that a mesh axis runs over, the one named last changes fastest.
Arguments:
- prompt: bfloat16 [4, 4096, 4096], P(None, 'sp'), may hold values from -6 to 6
- key_weight: bfloat16 [4096, 1024], P(None, 'tp'), may hold values from -0.09375 to 0.09375
- value_weight: bfloat16 [4096, 2048], P(None, 'tp'), may hold values from -0.09375 to 0.09375
- input_gate_weight: bfloat16 [4096, 16], P(None, 'tp'), may hold values from -0.09375 to 0.09375
- forget_gate_weight: bfloat16 [4096, 16], P(None, 'tp'), may hold values from -0.09375 to 0.09375
- forget_bias: float32 [16], P('tp'), may hold values from 3 to 11
- key_taps: bfloat16 [3, 1024], P(None, 'tp'), may hold values from -3 to 3
- extra_decay: float32 [4, 4096, 16], P(None, 'sp', 'tp'), may hold values from -1.5 to 0
- new_query: bfloat16 [4, 16, 64], P(None, 'tp'), may hold values from -6 to 6
- new_key: bfloat16 [4, 16, 64], P(None, 'tp'), may hold values from -6 to 6
- new_value: bfloat16 [4, 16, 128], P(None, 'tp', 'sp'), may hold values from -6 to 6
- new_input_gate: float32 [4, 16], P(None, 'tp'), may hold values from 2 to 7
- new_forget_gate: float32 [4, 16], P(None, 'tp'), may hold values from -2 to 4
- out_weight: bfloat16 [16, 128, 4096], P('tp', 'sp'), may hold values from -0.125 to 0.125
Outputs:
- cache_memory: bfloat16 [4, 16, 64, 128], P(None, 'tp', None, 'sp')
- cache_norm: bfloat16 [4, 16, 64], P(None, 'tp', 'sp')
- cache_peak: float32 [4, 16], P(None, 'tp')
- read_out: bfloat16 [4, 4096], P(None, ('sp', 'tp'))
All inputs are finite; a program needn't handle non-finite values.
Results may differ from a plain program's by a relative error of at most 0.012.
The roundings to bfloat16 on the way count: a program that leaves them out, or rounds other values in their place, can miss the bound.
Values may be sent and summed in bfloat16 or wider, within the bound.
A program may use at most 64 MiB of HBM per device.

v0:
```python
import jax
import jax.numpy as jnp
from jax import lax
from jax.sharding import PartitionSpec as P

KEY_DIM = 64


def with_halo(shard, sides, width):
    for axis, dim in sides:
        devices, length = (lax.axis_size(axis), shard.shape[dim])
        up = [(i, (i + 1) % devices) for i in range(devices - 1)]
        down = [(j, i) for i, j in up]
        last = lax.slice_in_dim(shard, length - width, length, axis=dim)
        leading = lax.slice_in_dim(shard, 0, width, axis=dim)
        before = lax.ppermute(last, axis, up)
        after = lax.ppermute(leading, axis, down)
        shard = jnp.concatenate([before, shard, after], axis=dim)
    return shard


def carried_in(shard, axis, combine, identity):
    devices, here = (lax.axis_size(axis), lax.axis_index(axis))
    everything = lax.all_gather(shard, axis)
    start = jnp.broadcast_to(jnp.asarray(identity, shard.dtype), shard.shape)

    def hop(k, before):
        at = devices - 1 - k
        reached = at > here
        new = combine(before, everything[at])
        return jnp.where(reached, new, before)

    return lax.fori_loop(0, devices, hop, start)


def widen(rounded):
    return lax.optimization_barrier(rounded).astype(jnp.float32)


def project(seq_rows, key_weight, value_weight, input_gate_weight, forget_gate_weight):
    seq_count, pos_count, width = seq_rows.shape
    flat_rows = seq_rows.reshape(seq_count * pos_count, width)
    key_raw = jnp.dot(flat_rows, key_weight, preferred_element_type=jnp.float32).astype(
        jnp.bfloat16
    )
    values = jnp.dot(flat_rows, value_weight, preferred_element_type=jnp.float32).astype(
        jnp.bfloat16
    )
    gate_weight = jnp.concatenate([input_gate_weight, forget_gate_weight], axis=1)
    gate_pre = jnp.dot(flat_rows, gate_weight, preferred_element_type=jnp.float32).astype(
        jnp.bfloat16
    )
    return (
        key_raw.reshape(seq_count, pos_count, -1),
        values.reshape(seq_count, pos_count, -1),
        gate_pre.reshape(seq_count, pos_count, -1),
    )


def key_conv(padded, key_taps):
    tap_f32 = key_taps.astype(jnp.float32)
    mixed = tap_f32[0] * padded[:, :-2] + tap_f32[1] * padded[:, 1:-1] + tap_f32[2] * padded[:, 2:]
    return (jax.nn.silu(mixed) * KEY_DIM ** (-0.5)).astype(jnp.bfloat16)


def gate_parts(gate_pre, forget_bias, extra):
    head_count = extra.shape[-1]
    gate_f32 = widen(gate_pre)
    input_pre = gate_f32[..., :head_count]
    log_forget = jax.nn.log_sigmoid(gate_f32[..., head_count:] + forget_bias) + extra
    return (input_pre, log_forget)


def suffix_of(log_forget):
    return jnp.sum(log_forget, axis=1, keepdims=True) - jnp.cumsum(log_forget, axis=1)


def add_later(earlier, latter):
    return earlier + latter


def body(
    prompt,
    key_weight,
    value_weight,
    input_gate_weight,
    forget_gate_weight,
    forget_bias,
    key_taps,
    extra_decay,
    new_query,
    new_key,
    new_value,
    new_input_gate,
    new_forget_gate,
    out_weight,
):
    seq_count = prompt.shape[0]
    head_count = extra_decay.shape[-1]
    key_size = new_key.shape[2]
    sp_count = lax.axis_size("sp")
    sp_index = lax.axis_index("sp")
    key_cols = key_size // sp_count
    key_raw, values, gate_pre = project(
        prompt, key_weight, value_weight, input_gate_weight, forget_gate_weight
    )
    input_pre, log_forget = gate_parts(gate_pre, forget_bias, extra_decay)
    padded = with_halo(key_raw, (("sp", 1),), 1)
    key_rows = key_conv(padded, key_taps)
    seg_total = jnp.sum(log_forget, axis=1)
    later_sum = carried_in(seg_total, "sp", add_later, jnp.zeros_like(seg_total))
    gate_log = input_pre + suffix_of(log_forget) + later_sum[:, None, :]
    peak_log = lax.pmax(jnp.max(gate_log, axis=1), "sp")
    scale = jnp.exp(gate_log - peak_log[:, None, :])
    pos_count = scale.shape[1]
    key_quartet = key_rows.reshape(seq_count, pos_count, head_count, key_size)
    value_four = values.reshape(seq_count, pos_count, head_count, -1)
    weighted_rows = (value_four * scale[..., None]).astype(jnp.bfloat16)
    memory_part = jnp.einsum(
        "slhk,slhv->shkv", key_quartet, weighted_rows, preferred_element_type=jnp.float32
    )
    normer_part = jnp.einsum(
        "slh,slhk->shk", scale, key_quartet.astype(jnp.float32), precision=lax.Precision.HIGHEST
    )
    memory_matrix, normer = (
        lax.psum_scatter(memory_part, "sp", scatter_dimension=3, tiled=True),
        lax.psum_scatter(normer_part, "sp", scatter_dimension=2, tiled=True),
    )
    forget_new = jax.nn.log_sigmoid(new_forget_gate)
    new_peak = jnp.maximum(forget_new + peak_log, new_input_gate)
    old_scale = jnp.exp(forget_new + peak_log - new_peak)
    new_scale = jnp.exp(new_input_gate - new_peak)
    key_new = new_key.astype(jnp.float32)
    key_new_slice = lax.dynamic_slice_in_dim(key_new, sp_index * key_cols, key_cols, 2)
    value_new = new_value.astype(jnp.float32)
    memory_next = (
        old_scale[:, :, None, None] * memory_matrix
        + new_scale[:, :, None, None] * key_new[:, :, :, None] * value_new[:, :, None, :]
    )
    normer_next = old_scale[:, :, None] * normer + new_scale[:, :, None] * key_new_slice
    query = new_query.astype(jnp.float32)
    query_slice = lax.dynamic_slice_in_dim(query, sp_index * key_cols, key_cols, 2)
    numer = jnp.sum(query[:, :, :, None] * memory_next, axis=2)
    denom = lax.psum(jnp.sum(query_slice * normer_next, axis=-1), "sp")
    read = (numer / jnp.maximum(jnp.abs(denom), 1.0)[:, :, None]).astype(jnp.bfloat16)
    partial_value = jnp.einsum("shv,hvd->sd", read, out_weight, preferred_element_type=jnp.float32)
    read_out = lax.psum_scatter(
        partial_value, ("sp", "tp"), scatter_dimension=1, tiled=True
    ).astype(jnp.bfloat16)
    return (memory_matrix.astype(jnp.bfloat16), normer.astype(jnp.bfloat16), peak_log, read_out)


def solution(mesh):
    placed = (
        P(None, "sp", None),
        P(None, "tp"),
        P(None, "tp"),
        P(None, "tp"),
        P(None, "tp"),
        P("tp"),
        P(None, "tp"),
        P(None, "sp", "tp"),
        P(None, "tp", None),
        P(None, "tp", None),
        P(None, "tp", "sp"),
        P(None, "tp"),
        P(None, "tp"),
        P("tp", "sp", None),
    )
    return jax.shard_map(
        body,
        mesh=mesh,
        in_specs=placed,
        out_specs=(
            P(None, "tp", None, "sp"),
            P(None, "tp", "sp"),
            P(None, "tp"),
            P(None, ("sp", "tp")),
        ),
        check_vma=False,
    )
```

profile of v0, /device:TPU:0, one launch (start us, length us, event | category | flops | bytes accessed | tf_op | source)
XLA Modules:
  0.0 337.2 jit_solution(1434747323576599410)
XLA Ops:
  7.2 1.5 copy-done
  8.8 8.2 %convolution_convert_fusion.1 = bf16[2048,256]{1,0:T(8,128)(2,1)S(1)} fusion(bf16[2048,4096]{1,0:T(8,128)(2,1)} %bitcast.42, bf16[4096,256]{1,0:T(8,128)(2,1)S(1)} %copy-done), kind=kOutput, calls=%fused_computation.5 | convolution fusion | flops 4295491584 | bytes 19922944 | tf_op jit(solution)/shard_map/dot_general | solution.py:43
  17.0 1.1 copy-done.2
  18.1 1.3 collective-permute-start.1
  19.4 5.5 %collective-permute-start = (bf16[4,1,256]{2,1,0:T(2,128)(2,1)S(1)}, bf16[4,1,256]{2,1,0:T(2,128)(2,1)S(1)}, u32[]{:S(2)}, u32[]{:S(2)}) collective-permute-start(bf16[4,1,256]{2,1,0:T(2,128)(2,1)S(1)} %get-tuple-element.140), channel_id=1, source_target_pairs={{0,4},{4,8},{8,12},{12,16},{16,20},{20,24},{24,28},{1,5},{5,9},{9,... | collective-permute-start | bytes 6152 | tf_op jit(solution)/shard_map/ppermute | solution.py:16
  25.0 10.2 %convolution_convert_fusion.2 = bf16[8,2048]{1,0:T(8,128)(2,1)S(1)} fusion(bf16[2048,4096]{1,0:T(8,128)(2,1)} %bitcast.43, bf16[4096,4]{0,1:T(4,128)(2,1)S(1)} %copy-done.3, bf16[4096,4]{0,1:T(4,128)(2,1)S(1)} %copy-done.4), kind=kOutput, calls=%fused_computation.6 | convolution fusion | flops 134365184 | bytes 16875520 | tf_op jit(solution)/shard_map/dot_general | solution.py:50
  35.4 27.0 %all-gather.1 = f32[8,4,4]{2,1,0:T(4,128)S(1)} all-gather(f32[1,4,4]{2,1,0:T(4,128)S(1)} %bitcast.53), channel_id=2, replica_groups=mesh['sp'=8,'tp'=4] {'sp'}, dimensions={0}, use_global_device_ids=true | all-gather | bytes 576 | tf_op jit(solution)/shard_map/all_gather | solution.py:24
  62.7 4.8 %reduce-window.6 = f32[4,4,4,128]{3,2,1,0:T(4,128)S(1)} reduce-window(f32[4,4,4,128]{3,2,1,0:T(4,128)S(1)} %reshape.55, f32[]{:T(128)} %constant.67.clone.1), window={size=1x1x1x128 pad=0_0x0_0x0_0x127_0}, to_apply=%region_1.2 | reduce-window | flops 1040384 | bytes 65540 | tf_op jit(solution)/shard_map/reduce-window
  67.8 0.7 reduce-window.9
  68.7 14.8 %fusion = f32[2048,512]{1,0:T(8,128)} fusion(bf16[2048,4096]{1,0:T(8,128)(2,1)} %bitcast.44, bf16[4096,512]{1,0:T(8,128)(2,1)} %param.18), kind=kOutput, calls=%fused_computation.4 | convolution fusion | flops 8592031744 | bytes 25165824 | tf_op jit(solution)/shard_map/dot_general | solution.py:46
  83.6 19.5 %pmax.7 = f32[4,4]{1,0:T(4,128)S(1)} all-reduce(f32[4,4]{1,0:T(4,128)S(1)} %fusion.18), channel_id=1, replica_groups=mesh['sp'=8,'tp'=4] {'sp'}, use_global_device_ids=true, to_apply=%region_6.7 | all-reduce | flops 16 | bytes 128 | tf_op jit(solution)/shard_map/pmax | solution.py:113
  103.2 5.2 %reshape.57 = f32[4,512,4,128]{3,2,1,0:T(4,128)} reshape(f32[2048,512]{1,0:T(8,128)} %fusion) | data formatting | bytes 8388608 | tf_op jit(solution)/shard_map/convert_element_type | solution.py:118
  108.5 5.2 %copy.23 = f32[4,512,4,128]{1,3,2,0:T(8,128)} copy(f32[4,512,4,128]{3,2,1,0:T(4,128)} %reshape.57) | data formatting | bytes 8388608 | tf_op jit(solution)/shard_map/convert_element_type | solution.py:118
  113.7 3.7 %multiply_convert_fusion.2 = bf16[4,512,256]{2,1,0:T(8,128)(2,1)S(1)} fusion(bf16[4,512,256]{2,1,0:T(8,128)(2,1)} %bitcast.48, bf16[4,1,256]{2,1,0:T(2,128)(2,1)S(1)} %collective-permute-done.1, bf16[4,1,256]{2,1,0:T(2,128)(2,1)S(1)} %collective-permute-done, f32[256]{0:T(256)S(1)} %bitcast.58, f32[256]{0:T(256)S(1)} %bitcast.57, f32[256]{0:T(256)S(1)} %bitcast.56), kind=kLoop, calls=%fused_computation.9 | loop fusion | flops 10485760 | bytes 2104320 | tf_op jit(solution)/shard_map/convert_element_type | solution.py:63
  117.4 1.3 copy.22
  118.8 4.3 %fusion.1 = f32[4,4,64,128]{2,3,1,0:T(8,128)} fusion(bf16[4,512,4,64]{1,3,2,0:T(8,128)(2,1)} %bitcast.45, f32[4,512,4,128]{1,3,2,0:T(8,128)} %copy.23, f32[4,512,4]{1,2,0:T(4,128)S(1)} %subtract_exponential_fusion), kind=kOutput, calls=%fused_computation.7 | convolution fusion | flops 136314880 | bytes 5799936 | tf_op jit(solution)/shard_map/slhk,slhv->shkv/dot_general | solution.py:119
  124.6 0.9 fusion.10
  125.5 17.6 %all-reduce = f32[4,4,64]{2,1,0:T(4,128)S(1)} all-reduce(f32[4,4,64]{2,1,0:T(4,128)S(1)} %bitcast.55), channel_id=4, replica_groups=mesh['sp'=8,'tp'=4] {'sp'}, use_global_device_ids=true, to_apply=%region_8.9.clone | all-reduce | flops 1024 | bytes 8192
  143.4 19.2 %psum.7 = f32[4,4]{1,0:T(4,128)S(1)} all-reduce(f32[4,4]{1,0:T(4,128)S(1)} %multiply_reduce_fusion.1), channel_id=1, replica_groups=mesh['sp'=8,'tp'=4] {'sp'}, use_global_device_ids=true, to_apply=%region_11.12 | all-reduce | flops 16 | bytes 128 | tf_op jit(solution)/shard_map/psum | solution.py:144
  162.6 22.6 %reduce-scatter.6.cloned.1.call-done = f32[4,4,64,16]{2,3,1,0:T(8,128)} async-done(((f32[4,4,64,128]{2,3,1,0:T(8,128)}), f32[4,4,64,16]{2,3,1,0:T(8,128)}) %reduce-scatter.6.cloned.1.call-update) | async-done | bytes 65552 | tf_op jit(solution)/shard_map/reduce_scatter | solution.py:126
  185.2 1.8 multiply_reduce_fusion
  187.0 4.1 %convolution_bitcast_fusion = f32[4096,4]{1,0:T(8,128)} fusion(bf16[4,16,4096]{2,1,0:T(8,128)(2,1)} %param.29, bf16[4,4,16]{2,1,0:T(4,128)(2,1)S(1)} %divide_convert_fusion), kind=kOutput, calls=%fused_computation.1 | convolution fusion | flops 2097152 | bytes 590336 | tf_op jit(solution)/shard_map/shv,hvd->sd/dot_general | solution.py:146
  191.8 137.0 %reduce-scatter.8.cloned.1.call-done = f32[128,4]{1,0:T(8,128)} async-done(((f32[4096,4]{1,0:T(8,128)}), f32[128,4]{1,0:T(8,128)}) %reduce-scatter.8.cloned.1.call-update) | async-done | bytes 2064
  328.9 1.5 copy.30
  (64 shorter events, 3.1 us)
Async XLA Ops:
  7.2 1.6 copy-start
  7.2 178.0 %reduce-scatter.6.cloned.1.call-start = ((), (), s32[]{:S(2)}) async-start(), calls=%async_computation.2 | async-start | bytes 1179648 | tf_op jit(solution)/shard_map/reduce_scatter | solution.py:126
  8.8 16.2 %copy-start.3 = (bf16[4096,4]{0,1:T(4,128)(2,1)S(1)}, bf16[4096,4]{0,1:T(4,128)(2,1)}, u32[]{:S(2)}) copy-start(bf16[4096,4]{0,1:T(4,128)(2,1)} %param.20) | copy-start | bytes 98308
  8.8 16.2 %copy-start.4 = (bf16[4096,4]{0,1:T(4,128)(2,1)S(1)}, bf16[4096,4]{0,1:T(4,128)(2,1)}, u32[]{:S(2)}) copy-start(bf16[4096,4]{0,1:T(4,128)(2,1)} %param.19) | copy-start | bytes 98308
  17.0 1.1 copy-start.2
  18.1 95.6 %collective-permute-start.1 = (bf16[4,1,256]{2,1,0:T(2,128)(2,1)S(1)}, bf16[4,1,256]{2,1,0:T(2,128)(2,1)S(1)}, u32[]{:S(2)}, u32[]{:S(2)}) collective-permute-start(bf16[4,1,256]{2,1,0:T(2,128)(2,1)S(1)} %get-tuple-element.141), channel_id=1, source_target_pairs={{4,0},{8,4},{12,8},{16,12},{20,16},{24,20},{28,24},{5,1},{9,5},{13... | collective-permute-start | bytes 6152 | tf_op jit(solution)/shard_map/ppermute | solution.py:17
  19.4 94.3 %collective-permute-start = (bf16[4,1,256]{2,1,0:T(2,128)(2,1)S(1)}, bf16[4,1,256]{2,1,0:T(2,128)(2,1)S(1)}, u32[]{:S(2)}, u32[]{:S(2)}) collective-permute-start(bf16[4,1,256]{2,1,0:T(2,128)(2,1)S(1)} %get-tuple-element.140), channel_id=1, source_target_pairs={{0,4},{4,8},{8,12},{12,16},{16,20},{20,24},{24,28},{1,5},{5,9},{9,... | collective-permute-start | bytes 6152 | tf_op jit(solution)/shard_map/ppermute | solution.py:16
  24.9 10.2 %copy-start.5 = (f32[4,512,4]{1,2,0:T(4,128)S(1)}, f32[4,512,4]{1,2,0:T(4,128)}, u32[]{:S(2)}) copy-start(f32[4,512,4]{1,2,0:T(4,128)} %param.23) | copy-start | bytes 98308
  25.0 10.2 %copy-start.13 = (f32[4]{0:T(128)S(1)}, f32[4]{0:T(128)}, u32[]{:S(2)}) copy-start(f32[4]{0:T(128)} %param.21) | copy-start | bytes 52
  68.7 34.5 %copy-start.8 = (bf16[3,256]{1,0:T(4,128)(2,1)S(1)}, bf16[3,256]{1,0:T(4,128)(2,1)}, u32[]{:S(2)}) copy-start(bf16[3,256]{1,0:T(4,128)(2,1)} %param.22) | copy-start | bytes 4612
  103.1 21.4 %copy-start.6 = (f32[4,4]{1,0:T(4,128)}, f32[4,4]{1,0:T(4,128)S(1)}, u32[]{:S(2)}) copy-start(f32[4,4]{1,0:T(4,128)S(1)} %pmax.7) | copy-start | bytes 196
  118.8 4.4 %copy-start.9 = (bf16[4,4,64]{2,1,0:T(4,128)(2,1)S(1)}, bf16[4,4,64]{2,1,0:T(4,128)(2,1)}, u32[]{:S(2)}) copy-start(bf16[4,4,64]{2,1,0:T(4,128)(2,1)} %param.24) | copy-start | bytes 6148
  118.8 4.4 %copy-start.7 = (bf16[4,4,64]{2,1,0:T(4,128)(2,1)S(1)}, bf16[4,4,64]{2,1,0:T(4,128)(2,1)}, u32[]{:S(2)}) copy-start(bf16[4,4,64]{2,1,0:T(4,128)(2,1)} %param.25) | copy-start | bytes 6148
  118.8 4.5 %copy-start.14 = (u32[32]{0:T(128)S(1)}, u32[32]{0:T(128)}, u32[]{:S(2)}) copy-start(u32[32]{0:T(128)} %constant.76) | copy-start | bytes 388
  118.8 5.7 %copy-start.11 = (f32[4,4]{1,0:T(4,128)S(1)}, f32[4,4]{1,0:T(4,128)}, u32[]{:S(2)}) copy-start(f32[4,4]{1,0:T(4,128)} %param.27) | copy-start | bytes 196
  118.8 5.7 %copy-start.12 = (f32[4,4]{1,0:T(4,128)S(1)}, f32[4,4]{1,0:T(4,128)}, u32[]{:S(2)}) copy-start(f32[4,4]{1,0:T(4,128)} %param.28) | copy-start | bytes 196
  118.8 5.8 %copy-start.1 = (bf16[4,512,256]{1,2,0:T(8,128)(2,1)S(1)}, bf16[4,512,256]{1,2,0:T(8,128)(2,1)}, u32[]{:S(2)}) copy-start(bf16[4,512,256]{1,2,0:T(8,128)(2,1)} %copy.22) | copy-start | bytes 3145732
  123.1 20.3 %copy-start.10 = (bf16[4,4,16]{2,1,0:T(4,128)(2,1)S(1)}, bf16[4,4,16]{2,1,0:T(4,128)(2,1)}, u32[]{:S(2)}) copy-start(bf16[4,4,16]{2,1,0:T(4,128)(2,1)} %param.26) | copy-start | bytes 1540
  123.1 205.7 %reduce-scatter.8.cloned.1.call-start = ((), (), s32[]{:S(2)}) async-start(), calls=%async_computation.3 | async-start | bytes 2162688
Sparse Core Ops, SparseCore 0:
  123.3 61.9 reduce-scatter.5
  191.3 137.5 reduce-scatter.7
where the time goes:
time: 338 us; the launch traced here: 337 us
  waiting for transfers between devices  160 us (47%)
  blocking collectives  83.3 us (25%)
  matrix products  42.6 us (13%)
  local copies, waits for them, and re-layouts  17.5 us (5%)
  between operations  15 us (4%)
  other arithmetic  12.1 us (4%)
  starting transfers between devices  6.87 us (2%)
    unnamed x3, waiting for transfers between devices  137 us
    all_gather x1, blocking collectives, carried_in(): everything = lax.all_gather(shard, axis)  27 us
    reduce_scatter x1, waiting for transfers between devices, body(): lax.psum_scatter(memory_part, 'sp', scatter_dimension=3, tiled=True)  22.6 us
    pmax x1, blocking collectives, body(): peak_log = lax.pmax(jnp.max(gate_log, axis=1), 'sp')  19.5 us
    psum x1, blocking collectives, body(): denom = lax.psum(jnp.sum(query_slice * normer_next, axis=-1), 'sp')  19.2 us
    unnamed x1, blocking collectives  17.6 us
    dot_general x1, matrix products, project(): jnp.dot(flat_rows, value_weight, preferred_element_type=jnp.float32)  14.8 us
    convert_element_type x2, local copies, waits for them, and re-layouts, body(): weighted_rows = (value_four * scale[..., None]).astype(jnp.bfloat16)  10.5 us
  transfers between devices with their start and end apart: 4, of which 2 were waited for; matrix products, arithmetic and copies ran while one was open for 13% of the time, Pallas kernels for 0%

commit v1 on v0

--- a/solution.py
+++ b/solution.py
@@ -141,7 +141,9 @@
     query = new_query.astype(jnp.float32)
     query_slice = lax.dynamic_slice_in_dim(query, sp_index * key_cols, key_cols, 2)
     numer = jnp.sum(query[:, :, :, None] * memory_next, axis=2)
-    denom = lax.psum(jnp.sum(query_slice * normer_next, axis=-1), "sp")
+    part = jnp.sum(query_slice * normer_next, axis=-1)
+    shards = lax.all_gather(part, "sp")
+    denom = jnp.sum(shards, axis=0)
     read = (numer / jnp.maximum(jnp.abs(denom), 1.0)[:, :, None]).astype(jnp.bfloat16)
     partial_value = jnp.einsum("shv,hvd->sd", read, out_weight, preferred_element_type=jnp.float32)
     read_out = lax.psum_scatter(

time: 338 us -> 338 us (level)
  blocking collectives: 83.3 us -> 90.3 us
  waiting for transfers between devices: 160 us -> 153 us
    all_gather x0 -> x1, blocking collectives: none -> 26.2 us  [body(): shards = lax.all_gather(part, 'sp')]
    psum x1 -> x0, blocking collectives: 19.2 us -> none  [body(): denom = lax.psum(jnp.sum(query_slice * normer_next, axis=-1), 'sp')]
    reduce_scatter x1, waiting for transfers between devices: 22.6 us -> 15.6 us  [body(): lax.psum_scatter(memory_part, 'sp', scatter_dimension=3, tiled=True)]
where the time goes in v1:
time: 338 us; the launch traced here: 337 us
  waiting for transfers between devices  153 us (45%)
  blocking collectives  90.3 us (27%)
  matrix products  42.6 us (13%)
  local copies, waits for them, and re-layouts  17.5 us (5%)
  between operations  15 us (4%)
  other arithmetic  12.1 us (4%)
  starting transfers between devices  6.87 us (2%)
    unnamed x3, waiting for transfers between devices  137 us
    all_gather x1, blocking collectives, carried_in(): everything = lax.all_gather(shard, axis)  27 us
    all_gather x1, blocking collectives, body(): shards = lax.all_gather(part, 'sp')  26.2 us
    pmax x1, blocking collectives, body(): peak_log = lax.pmax(jnp.max(gate_log, axis=1), 'sp')  19.5 us
    unnamed x1, blocking collectives  17.6 us
    reduce_scatter x1, waiting for transfers between devices, body(): lax.psum_scatter(memory_part, 'sp', scatter_dimension=3, tiled=True)  15.6 us
    dot_general x1, matrix products, project(): jnp.dot(flat_rows, value_weight, preferred_element_type=jnp.float32)  14.8 us
    convert_element_type x2, local copies, waits for them, and re-layouts, body(): weighted_rows = (value_four * scale[..., None]).astype(jnp.bfloat16)  10.5 us
  transfers between devices with their start and end apart: 4, of which 2 were waited for; matrix products, arithmetic and copies ran while one was open for 13% of the time, Pallas kernels for 0%

profile of v1, /device:TPU:0, one launch (start us, length us, event | category | flops | bytes accessed | tf_op | source)
XLA Modules:
  0.0 337.2 jit_solution(16985457034822607928)
XLA Ops:
  7.2 1.5 copy-done
  8.8 8.2 %convolution_convert_fusion.1 = bf16[2048,256]{1,0:T(8,128)(2,1)S(1)} fusion(bf16[2048,4096]{1,0:T(8,128)(2,1)} %bitcast.43, bf16[4096,256]{1,0:T(8,128)(2,1)S(1)} %copy-done), kind=kOutput, calls=%fused_computation.5 | convolution fusion | flops 4295491584 | bytes 19922944 | tf_op jit(solution)/shard_map/dot_general | solution.py:43
  17.0 1.1 copy-done.2
  18.1 1.3 collective-permute-start.1
  19.4 5.5 %collective-permute-start = (bf16[4,1,256]{2,1,0:T(2,128)(2,1)S(1)}, bf16[4,1,256]{2,1,0:T(2,128)(2,1)S(1)}, u32[]{:S(2)}, u32[]{:S(2)}) collective-permute-start(bf16[4,1,256]{2,1,0:T(2,128)(2,1)S(1)} %get-tuple-element.140), channel_id=1, source_target_pairs={{0,4},{4,8},{8,12},{12,16},{16,20},{20,24},{24,28},{1,5},{5,9},{9,... | collective-permute-start | bytes 6152 | tf_op jit(solution)/shard_map/ppermute | solution.py:16
  25.0 10.2 %convolution_convert_fusion.2 = bf16[8,2048]{1,0:T(8,128)(2,1)S(1)} fusion(bf16[2048,4096]{1,0:T(8,128)(2,1)} %bitcast.44, bf16[4096,4]{0,1:T(4,128)(2,1)S(1)} %copy-done.3, bf16[4096,4]{0,1:T(4,128)(2,1)S(1)} %copy-done.4), kind=kOutput, calls=%fused_computation.6 | convolution fusion | flops 134365184 | bytes 16875520 | tf_op jit(solution)/shard_map/dot_general | solution.py:50
  35.4 27.0 %all-gather.2 = f32[8,4,4]{2,1,0:T(4,128)S(1)} all-gather(f32[1,4,4]{2,1,0:T(4,128)S(1)} %bitcast.54), channel_id=2, replica_groups=mesh['sp'=8,'tp'=4] {'sp'}, dimensions={0}, use_global_device_ids=true | all-gather | bytes 576 | tf_op jit(solution)/shard_map/all_gather | solution.py:24
  62.7 4.8 %reduce-window.6 = f32[4,4,4,128]{3,2,1,0:T(4,128)S(1)} reduce-window(f32[4,4,4,128]{3,2,1,0:T(4,128)S(1)} %reshape.58, f32[]{:T(128)} %constant.67.clone.1), window={size=1x1x1x128 pad=0_0x0_0x0_0x127_0}, to_apply=%region_1.2 | reduce-window | flops 1040384 | bytes 65540 | tf_op jit(solution)/shard_map/reduce-window
  67.8 0.7 reduce-window.9
  68.7 14.8 %fusion = f32[2048,512]{1,0:T(8,128)} fusion(bf16[2048,4096]{1,0:T(8,128)(2,1)} %bitcast.45, bf16[4096,512]{1,0:T(8,128)(2,1)} %param.18), kind=kOutput, calls=%fused_computation.4 | convolution fusion | flops 8592031744 | bytes 25165824 | tf_op jit(solution)/shard_map/dot_general | solution.py:46
  83.6 19.5 %pmax.7 = f32[4,4]{1,0:T(4,128)S(1)} all-reduce(f32[4,4]{1,0:T(4,128)S(1)} %fusion.18), channel_id=1, replica_groups=mesh['sp'=8,'tp'=4] {'sp'}, use_global_device_ids=true, to_apply=%region_6.7 | all-reduce | flops 16 | bytes 128 | tf_op jit(solution)/shard_map/pmax | solution.py:113
  103.2 5.2 %reshape.60 = f32[4,512,4,128]{3,2,1,0:T(4,128)} reshape(f32[2048,512]{1,0:T(8,128)} %fusion) | data formatting | bytes 8388608 | tf_op jit(solution)/shard_map/convert_element_type | solution.py:118
  108.5 5.2 %copy.23 = f32[4,512,4,128]{1,3,2,0:T(8,128)} copy(f32[4,512,4,128]{3,2,1,0:T(4,128)} %reshape.60) | data formatting | bytes 8388608 | tf_op jit(solution)/shard_map/convert_element_type | solution.py:118
  113.7 3.7 %multiply_convert_fusion.2 = bf16[4,512,256]{2,1,0:T(8,128)(2,1)S(1)} fusion(bf16[4,512,256]{2,1,0:T(8,128)(2,1)} %bitcast.49, bf16[4,1,256]{2,1,0:T(2,128)(2,1)S(1)} %collective-permute-done.1, bf16[4,1,256]{2,1,0:T(2,128)(2,1)S(1)} %collective-permute-done, f32[256]{0:T(256)S(1)} %bitcast.60, f32[256]{0:T(256)S(1)} %bitcast.59, f32[256]{0:T(256)S(1)} %bitcast.58), kind=kLoop, calls=%fused_computation.9 | loop fusion | flops 10485760 | bytes 2104320 | tf_op jit(solution)/shard_map/convert_element_type | solution.py:63
  117.4 1.3 copy.22
  118.8 4.3 %fusion.1 = f32[4,4,64,128]{2,3,1,0:T(8,128)} fusion(bf16[4,512,4,64]{1,3,2,0:T(8,128)(2,1)} %bitcast.46, f32[4,512,4,128]{1,3,2,0:T(8,128)} %copy.23, f32[4,512,4]{1,2,0:T(4,128)S(1)} %subtract_exponential_fusion), kind=kOutput, calls=%fused_computation.7 | convolution fusion | flops 136314880 | bytes 5799936 | tf_op jit(solution)/shard_map/slhk,slhv->shkv/dot_general | solution.py:119
  124.7 0.9 fusion.10
  125.6 17.6 %all-reduce = f32[4,4,64]{2,1,0:T(4,128)S(1)} all-reduce(f32[4,4,64]{2,1,0:T(4,128)S(1)} %bitcast.57), channel_id=5, replica_groups=mesh['sp'=8,'tp'=4] {'sp'}, use_global_device_ids=true, to_apply=%region_8.9.clone | all-reduce | flops 1024 | bytes 8192
  143.4 26.2 %all-gather.3 = f32[8,4,4]{2,1,0:T(4,128)S(1)} all-gather(f32[1,4,4]{2,1,0:T(4,128)S(1)} %bitcast.56), channel_id=3, replica_groups=mesh['sp'=8,'tp'=4] {'sp'}, dimensions={0}, use_global_device_ids=true | all-gather | bytes 576 | tf_op jit(solution)/shard_map/all_gather | solution.py:145
  169.6 15.6 %reduce-scatter.6.cloned.1.call-done = f32[4,4,64,16]{2,3,1,0:T(8,128)} async-done(((f32[4,4,64,128]{2,3,1,0:T(8,128)}), f32[4,4,64,16]{2,3,1,0:T(8,128)}) %reduce-scatter.6.cloned.1.call-update) | async-done | bytes 65552 | tf_op jit(solution)/shard_map/reduce_scatter | solution.py:126
  185.2 1.8 multiply_reduce_fusion
  187.0 4.1 %convolution_bitcast_fusion = f32[4096,4]{1,0:T(8,128)} fusion(bf16[4,16,4096]{2,1,0:T(8,128)(2,1)} %param.29, bf16[4,4,16]{2,1,0:T(4,128)(2,1)S(1)} %divide_convert_fusion), kind=kOutput, calls=%fused_computation.1 | convolution fusion | flops 2097152 | bytes 590336 | tf_op jit(solution)/shard_map/shv,hvd->sd/dot_general | solution.py:148
  191.9 137.0 %reduce-scatter.8.cloned.1.call-done = f32[128,4]{1,0:T(8,128)} async-done(((f32[4096,4]{1,0:T(8,128)}), f32[128,4]{1,0:T(8,128)}) %reduce-scatter.8.cloned.1.call-update) | async-done | bytes 2064
  328.9 1.5 copy.30
  (65 shorter events, 3.1 us)
Async XLA Ops:
  7.2 1.6 copy-start
  7.2 178.0 %reduce-scatter.6.cloned.1.call-start = ((), (), s32[]{:S(2)}) async-start(), calls=%async_computation.2 | async-start | bytes 1179648 | tf_op jit(solution)/shard_map/reduce_scatter | solution.py:126
  8.8 16.2 %copy-start.3 = (bf16[4096,4]{0,1:T(4,128)(2,1)S(1)}, bf16[4096,4]{0,1:T(4,128)(2,1)}, u32[]{:S(2)}) copy-start(bf16[4096,4]{0,1:T(4,128)(2,1)} %param.20) | copy-start | bytes 98308
  8.8 16.2 %copy-start.4 = (bf16[4096,4]{0,1:T(4,128)(2,1)S(1)}, bf16[4096,4]{0,1:T(4,128)(2,1)}, u32[]{:S(2)}) copy-start(bf16[4096,4]{0,1:T(4,128)(2,1)} %param.19) | copy-start | bytes 98308
  17.0 1.1 copy-start.2
  18.1 95.6 %collective-permute-start.1 = (bf16[4,1,256]{2,1,0:T(2,128)(2,1)S(1)}, bf16[4,1,256]{2,1,0:T(2,128)(2,1)S(1)}, u32[]{:S(2)}, u32[]{:S(2)}) collective-permute-start(bf16[4,1,256]{2,1,0:T(2,128)(2,1)S(1)} %get-tuple-element.141), channel_id=1, source_target_pairs={{4,0},{8,4},{12,8},{16,12},{20,16},{24,20},{28,24},{5,1},{9,5},{13... | collective-permute-start | bytes 6152 | tf_op jit(solution)/shard_map/ppermute | solution.py:17
  19.4 94.3 %collective-permute-start = (bf16[4,1,256]{2,1,0:T(2,128)(2,1)S(1)}, bf16[4,1,256]{2,1,0:T(2,128)(2,1)S(1)}, u32[]{:S(2)}, u32[]{:S(2)}) collective-permute-start(bf16[4,1,256]{2,1,0:T(2,128)(2,1)S(1)} %get-tuple-element.140), channel_id=1, source_target_pairs={{0,4},{4,8},{8,12},{12,16},{16,20},{20,24},{24,28},{1,5},{5,9},{9,... | collective-permute-start | bytes 6152 | tf_op jit(solution)/shard_map/ppermute | solution.py:16
  24.9 10.2 %copy-start.5 = (f32[4,512,4]{1,2,0:T(4,128)S(1)}, f32[4,512,4]{1,2,0:T(4,128)}, u32[]{:S(2)}) copy-start(f32[4,512,4]{1,2,0:T(4,128)} %param.23) | copy-start | bytes 98308
  25.0 10.2 %copy-start.13 = (f32[4]{0:T(128)S(1)}, f32[4]{0:T(128)}, u32[]{:S(2)}) copy-start(f32[4]{0:T(128)} %param.21) | copy-start | bytes 52
  68.7 34.5 %copy-start.8 = (bf16[3,256]{1,0:T(4,128)(2,1)S(1)}, bf16[3,256]{1,0:T(4,128)(2,1)}, u32[]{:S(2)}) copy-start(bf16[3,256]{1,0:T(4,128)(2,1)} %param.22) | copy-start | bytes 4612
  103.1 21.4 %copy-start.6 = (f32[4,4]{1,0:T(4,128)}, f32[4,4]{1,0:T(4,128)S(1)}, u32[]{:S(2)}) copy-start(f32[4,4]{1,0:T(4,128)S(1)} %pmax.7) | copy-start | bytes 196
  118.8 4.4 %copy-start.9 = (bf16[4,4,16]{2,1,0:T(4,128)(2,1)S(1)}, bf16[4,4,16]{2,1,0:T(4,128)(2,1)}, u32[]{:S(2)}) copy-start(bf16[4,4,16]{2,1,0:T(4,128)(2,1)} %param.26) | copy-start | bytes 1540
  118.8 4.5 %copy-start.10 = (bf16[4,4,64]{2,1,0:T(4,128)(2,1)S(1)}, bf16[4,4,64]{2,1,0:T(4,128)(2,1)}, u32[]{:S(2)}) copy-start(bf16[4,4,64]{2,1,0:T(4,128)(2,1)} %param.24) | copy-start | bytes 6148
  118.8 4.5 %copy-start.7 = (bf16[4,4,64]{2,1,0:T(4,128)(2,1)S(1)}, bf16[4,4,64]{2,1,0:T(4,128)(2,1)}, u32[]{:S(2)}) copy-start(bf16[4,4,64]{2,1,0:T(4,128)(2,1)} %param.25) | copy-start | bytes 6148
  118.8 4.5 %copy-start.14 = (u32[32]{0:T(128)S(1)}, u32[32]{0:T(128)}, u32[]{:S(2)}) copy-start(u32[32]{0:T(128)} %constant.76) | copy-start | bytes 388
  118.8 5.8 %copy-start.11 = (f32[4,4]{1,0:T(4,128)S(1)}, f32[4,4]{1,0:T(4,128)}, u32[]{:S(2)}) copy-start(f32[4,4]{1,0:T(4,128)} %param.27) | copy-start | bytes 196
  118.8 5.8 %copy-start.12 = (f32[4,4]{1,0:T(4,128)S(1)}, f32[4,4]{1,0:T(4,128)}, u32[]{:S(2)}) copy-start(f32[4,4]{1,0:T(4,128)} %param.28) | copy-start | bytes 196
  118.8 5.9 %copy-start.1 = (bf16[4,512,256]{1,2,0:T(8,128)(2,1)S(1)}, bf16[4,512,256]{1,2,0:T(8,128)(2,1)}, u32[]{:S(2)}) copy-start(bf16[4,512,256]{1,2,0:T(8,128)(2,1)} %copy.22) | copy-start | bytes 3145732
  123.1 205.7 %reduce-scatter.8.cloned.1.call-start = ((), (), s32[]{:S(2)}) async-start(), calls=%async_computation.3 | async-start | bytes 2162688
Sparse Core Ops, SparseCore 0:
  123.3 61.9 reduce-scatter.5
  191.3 137.5 reduce-scatter.7
